TPU v7x, 256 devices: a 4x2x16 block of a 4x16x16 slice. The times are simulated.
256 devices in a mesh: grp: 2 (over y), ep: 64 (over z, x), tp: 2 (over core).
Axes of the slice: x: 4, y: 2, z: 16, core: 2. Of those that a mesh axis runs over, the one named last changes fastest.
The devices are a block of a 4x16x16 slice.
Arguments:
- tokens: bfloat16 [12288, 2048], P(('grp', 'ep')), parts along dimension 0, may hold values from -6 to 6
- prior_state: float32 [2, 12288, 4096], P(None, ('grp', 'ep'), 'tp'), parts along dimension 1, may hold values from -6 to 6
- mix_gain: float32 [2048], replicated, may hold values from 0.1 to 1.9
- in_weight: bfloat16 [2048, 1024], P(None, 'tp'), may hold values from -0.125 to 0.125
- decay_rate: float32 [64, 64], P('tp'), may hold values from 0.2 to 20
- frequency: float32 [64, 64], P('tp'), may hold values from 0 to 12
- log_step: float32 [64], P('tp'), may hold values from -4.6 to 0
- input_map: float32 [2, 64, 64, 16], P(None, 'tp'), may hold values from -6 to 6
- output_map: float32 [2, 64, 16, 64], P(None, 'tp'), may hold values from -0.5 to 0.5
- skip_gain: float32 [1024], P('tp'), may hold values from -4 to 4
- out_weight: bfloat16 [1024, 2048], P('tp'), may hold values from -0.1875 to 0.1875
- channel_gain: float32 [2048], replicated, may hold values from 0.1 to 1.9
- expert_gate: bfloat16 [64, 2048, 512], P('ep', None, 'tp'), may hold values from -0.125 to 0.125
- expert_up: bfloat16 [64, 2048, 512], P('ep', None, 'tp'), may hold values from -0.125 to 0.125
- expert_down: bfloat16 [64, 512, 2048], P('ep', 'tp'), may hold values from -0.25 to 0.25
- shared_gate: bfloat16 [2048, 512], P(None, 'tp'), may hold values from -0.125 to 0.125
- shared_up: bfloat16 [2048, 512], P(None, 'tp'), may hold values from -0.125 to 0.125
- shared_down: bfloat16 [512, 2048], P('tp'), may hold values from -0.25 to 0.25
- routes: int32 [12288, 6], P(('grp', 'ep')), parts along dimension 0, may hold values from 0 to 63, all different within a row; in each aligned block of 96 rows (0 to 95, 96 to 191, ...) at most 13 rows name the same one
- route_weights: float32 [12288, 6], P(('grp', 'ep')), parts along dimension 0, may hold values from 0.05 to 0.8
Outputs:
- layer_out: bfloat16 [12288, 2048], P(('grp', 'ep'), 'tp'), parts along dimension 0
- new_state: float32 [2, 12288, 4096], P(None, ('grp', 'ep'), 'tp'), parts along dimension 1
There are 2 independent parts, one for each index of `grp`. A program takes and returns all parts, laid end to end along the dimension named above; an argument that names none is the same for every part. Nothing has to cross between parts.
Inputs may be any that keep to these rules, and one draw needn't show every extreme that they name: `routes`: each row names 6 different experts; among the rows of one index of ep no expert is named by more than 13 rows.
All inputs are finite; a program needn't handle non-finite values.
Results may differ from a plain program's by a relative error of at most 0.017.
Values may be sent and summed in bfloat16 or wider, within the bound.
No kernel may reach another device: no remote copies, remote signals or barrier semaphores. Data moves between devices by JAX's collectives and lax.ppermute only.
A program may use at most 128 MiB of HBM per device.

v0:
```python
import jax
import jax.numpy as jnp
from jax import lax
from jax.sharding import PartitionSpec as P

norm_eps = 1e-06


def copy_for_each(value, axis):
    peers = lax.axis_size(axis)
    return lax.all_to_all(
        jnp.broadcast_to(value[None], (peers, *value.shape)), axis, 0, 0, tiled=True
    )


def of_everyone(value, axis):
    return copy_for_each(value, axis).astype(jnp.float32).sum(axis=0)


def in_blocks(value, dim, peers):
    before, after = (value.shape[:dim], value.shape[dim + 1 :])
    return jnp.moveaxis(value.reshape(*before, peers, -1, *after), dim, 0)


def summed_on_arrival(value, axis, dim):
    tiles = in_blocks(value, dim, lax.axis_size(axis))
    arrived = lax.all_to_all(tiles, axis, split_axis=0, concat_axis=0, tiled=True)
    return arrived.astype(jnp.float32).sum(axis=0)


def root_scale(activations, scale_gain):
    values = activations.astype(jnp.float32)
    factor = lax.rsqrt(jnp.mean(values * values, axis=-1, keepdims=True) + norm_eps)
    return (values * factor * scale_gain).astype(jnp.bfloat16)


def state_update(
    drive_rows, prior_state, decay_rate, frequency, log_step, input_map, output_map, skip_gain
):
    sequences = drive_rows.shape[0]
    groups = decay_rate.shape[0]
    driven = drive_rows.astype(jnp.float32).reshape(sequences, groups, -1)
    step_size = jnp.exp(log_step)[:, None]
    real_rate = -decay_rate
    magnitude = jnp.exp(real_rate * step_size)
    turn_real = magnitude * jnp.cos(frequency * step_size)
    turn_imag = magnitude * jnp.sin(frequency * step_size)
    denominator = real_rate * real_rate + frequency * frequency
    hold_real = ((turn_real - 1.0) * real_rate + turn_imag * frequency) / denominator
    hold_imag = (turn_imag * real_rate - (turn_real - 1.0) * frequency) / denominator
    push_real = jnp.einsum("sgh,gph->sgp", driven, input_map[0])
    push_imag = jnp.einsum("sgh,gph->sgp", driven, input_map[1])
    enter_real = push_real * hold_real - push_imag * hold_imag
    enter_imag = push_real * hold_imag + push_imag * hold_real
    old_real = prior_state[0].reshape(sequences, groups, -1)
    old_imag = prior_state[1].reshape(sequences, groups, -1)
    fresh_real = turn_real * old_real - turn_imag * old_imag + enter_real
    fresh_imag = turn_real * old_imag + turn_imag * old_real + enter_imag
    readout = jnp.einsum("ghp,sgp->sgh", output_map[0], fresh_real)
    readout = readout - jnp.einsum("ghp,sgp->sgh", output_map[1], fresh_imag)
    readout = readout.reshape(sequences, -1) + skip_gain * drive_rows.astype(jnp.float32)
    fresh = jnp.stack([fresh_real.reshape(sequences, -1), fresh_imag.reshape(sequences, -1)])
    return (readout, fresh)


def body(
    tokens,
    prior_state,
    mix_gain,
    in_weight,
    decay_rate,
    frequency,
    log_step,
    input_map,
    output_map,
    skip_gain,
    out_weight,
    channel_gain,
    expert_gate,
    expert_up,
    expert_down,
    shared_gate,
    shared_up,
    shared_down,
    routes,
    route_weights,
):
    normed = root_scale(tokens, mix_gain)
    drive_rows = jnp.dot(normed, in_weight, preferred_element_type=jnp.float32).astype(jnp.bfloat16)
    readout, new_state = state_update(
        drive_rows, prior_state, decay_rate, frequency, log_step, input_map, output_map, skip_gain
    )
    activated = jax.nn.gelu(readout).astype(jnp.bfloat16)
    partial_value = jnp.dot(activated, out_weight, preferred_element_type=jnp.float32)
    mixer_out = of_everyone(partial_value.astype(jnp.bfloat16), "tp").astype(jnp.float32)
    middle = (tokens.astype(jnp.float32) + mixer_out).astype(jnp.bfloat16)
    second_normed = root_scale(middle, channel_gain)
    shared_gval = jnp.dot(second_normed, shared_gate, preferred_element_type=jnp.float32)
    shared_uval = jnp.dot(second_normed, shared_up, preferred_element_type=jnp.float32)
    shared_hidden = (jax.nn.silu(shared_gval) * shared_uval).astype(jnp.bfloat16)
    shared_piece = jnp.dot(shared_hidden, shared_down, preferred_element_type=jnp.float32)
    shared_out = summed_on_arrival(shared_piece.astype(jnp.bfloat16), "tp", 1)
    experts = lax.axis_size("ep")
    seq_rows, top_count = routes.shape
    slot_cap = min(seq_rows, max(2, 3 * seq_rows * top_count // (2 * experts)))
    flat_routes = routes.reshape(-1)
    one_hot = (flat_routes[:, None] == jnp.arange(experts, dtype=jnp.int32)[None, :]).astype(
        jnp.int32
    )
    ranked = jnp.sum((jnp.cumsum(one_hot, axis=0) - one_hot) * one_hot, axis=1)
    slot_index = flat_routes * slot_cap + ranked
    placed = slot_index[:, None] == jnp.arange(experts * slot_cap, dtype=jnp.int32)[None, :]
    placed_rows = jnp.any(placed.reshape(seq_rows, top_count, experts * slot_cap), axis=1).astype(
        jnp.bfloat16
    )
    outgoing = lax.dot_general(
        placed_rows, second_normed, (((0,), (0,)), ((), ())), preferred_element_type=jnp.float32
    ).astype(jnp.bfloat16)
    outgoing = outgoing.reshape(experts, slot_cap, -1)
    half_cols = outgoing.shape[2] // lax.axis_size("tp")
    own_cols = lax.dynamic_slice_in_dim(outgoing, lax.axis_index("tp") * half_cols, half_cols, 2)
    arrived = lax.all_gather(
        lax.all_to_all(own_cols, "ep", split_axis=0, concat_axis=0, tiled=True),
        "tp",
        axis=2,
        tiled=True,
    )
    sources, count_items, full_width = arrived.shape
    expert_rows = arrived.reshape(sources * count_items, full_width)
    gate_val = jnp.dot(expert_rows, expert_gate[0], preferred_element_type=jnp.float32)
    up_val = jnp.dot(expert_rows, expert_up[0], preferred_element_type=jnp.float32)
    hidden = (jax.nn.silu(gate_val) * up_val).astype(jnp.bfloat16)
    piece = jnp.dot(hidden, expert_down[0], preferred_element_type=jnp.float32)
    summed = summed_on_arrival(
        piece.reshape(sources, count_items, full_width).astype(jnp.bfloat16), "tp", 2
    )
    returned = lax.all_to_all(
        summed.astype(jnp.bfloat16), "ep", split_axis=0, concat_axis=0, tiled=True
    )
    flat_back = returned.reshape(experts * slot_cap, -1)
    picked = (
        jnp.take(flat_back, slot_index, axis=0).reshape(seq_rows, top_count, -1).astype(jnp.float32)
    )
    routed = jnp.einsum("sk,skd->sd", route_weights, picked)
    own_middle = lax.dynamic_slice_in_dim(middle, lax.axis_index("tp") * half_cols, half_cols, 1)
    layer_out = (own_middle.astype(jnp.float32) + routed + shared_out).astype(jnp.bfloat16)
    return (layer_out, new_state)


def solution(mesh):
    in_specs = (
        P(("grp", "ep"), None),
        P(None, ("grp", "ep"), "tp"),
        P(),
        P(None, "tp"),
        P("tp", None),
        P("tp", None),
        P("tp"),
        P(None, "tp", None, None),
        P(None, "tp", None, None),
        P("tp"),
        P("tp", None),
        P(),
        P("ep", None, "tp"),
        P("ep", None, "tp"),
        P("ep", "tp", None),
        P(None, "tp"),
        P(None, "tp"),
        P("tp", None),
        P(("grp", "ep"), None),
        P(("grp", "ep"), None),
    )
    out_specs = (P(("grp", "ep"), "tp"), P(None, ("grp", "ep"), "tp"))
    return jax.shard_map(body, mesh=mesh, in_specs=in_specs, out_specs=out_specs, check_vma=False)
```

profile of v0, /device:TPU:34, one launch (start us, length us, event | category | flops | bytes accessed | tf_op | source)
XLA Modules:
  0.0 344.4 jit_solution(5603154047995699530)
XLA Ops:
  8.0 1.2 fusion.13
  9.2 2.3 convolution_convert_fusion.4
  11.6 2.7 fusion.72
  14.3 1.5 copy.89
  15.8 2.5 copy.90
  18.2 1.4 fusion.29
  19.8 3.0 bitcast_add_fusion
  25.8 3.7 %all-to-all-start = ((bf16[2,96,2048]{2,1,0:T(8,128)(2,1)}), bf16[2,96,2048]{2,1,0:T(8,128)(2,1)S(1)}, u32[]{:S(2)}, u32[]{:S(2)}) async-start(bf16[2,96,2048]{2,1,0:T(8,128)(2,1)} %broadcast_in_dim.9), calls=%async_computation | async-start | bytes 1572864 | tf_op jit(solution)/shard_map/all_to_all | solution.py:11
  29.9 1.5 reduce-window.6
  33.6 1.1 convolution_convert_fusion.1
  34.7 2.9 reshape.128
  37.6 1.8 constant_dynamic-slice_fusion
  39.4 128.1 %all_to_all.25 = bf16[64,13,1024]{2,1,0:T(8,128)(2,1)} all-to-all(bf16[64,13,1024]{2,1,0:T(8,128)(2,1)S(1)} %constant_dynamic-slice_fusion), channel_id=1, replica_groups=mesh['grp'=2,'ep'=64,'tp'=2] {'ep'}, dimensions={0} | all-to-all | bytes 3407872 | tf_op jit(solution)/shard_map/all_to_all | solution.py:123
  168.5 1.6 fusion.67
  171.7 10.8 %all-gather.2.cloned.1.call-done = bf16[64,13,2048]{2,1,0:T(8,128)(2,1)} async-done(((bf16[64,13,1024]{2,1,0:T(8,128)(2,1)}), bf16[64,13,2048]{2,1,0:T(8,128)(2,1)}) %all-gather.2.cloned.1.call-update) | async-done | bytes 3407888 | tf_op jit(solution)/shard_map/all_gather | solution.py:122
  182.5 3.4 reshape.129
  185.9 2.4 fusion.8
  188.3 1.8 fusion.4
  190.1 1.2 dot_general.53
  191.3 2.3 convolution_convert_fusion
  194.1 6.5 %all_to_all.26 = bf16[2,64,13,1024]{3,1,2,0:T(8,128)(2,1)S(1)} all-to-all(bf16[2,64,13,1024]{3,1,2,0:T(8,128)(2,1)S(1)} %bitcast.84), channel_id=1, replica_groups=mesh['grp'=2,'ep'=64,'tp'=2] {'tp'}, dimensions={0} | all-to-all | bytes 6815744 | tf_op jit(solution)/shard_map/all_to_all | solution.py:27
  200.6 4.2 %all-to-all-start.4 = ((bf16[2,96,1024]{2,1,0:T(8,128)(2,1)}), bf16[2,96,1024]{2,1,0:T(8,128)(2,1)}, u32[]{:S(2)}, u32[]{:S(2)}) async-start(bf16[2,96,1024]{2,1,0:T(8,128)(2,1)} %bitcast.89), calls=%async_computation.4 | async-start | bytes 786432 | tf_op jit(solution)/shard_map/all_to_all | solution.py:27
  204.8 2.5 reduce_sum.66
  207.2 3.7 %copy.101 = bf16[64,13,1024]{2,1,0:T(8,128)(2,1)} copy(bf16[64,13,1024]{2,0,1:T(8,128)(2,1)} %reduce_sum.66) | data formatting | bytes 3407872 | tf_op jit(solution)/shard_map/reduce_sum | solution.py:28
  211.0 16.5 %all-to-all-start.3 = ((bf16[64,13,1024]{2,1,0:T(8,128)(2,1)}), bf16[64,13,1024]{2,1,0:T(8,128)(2,1)}, u32[]{:S(2)}, u32[]{:S(2)}) async-start(bf16[64,13,1024]{2,1,0:T(8,128)(2,1)} %copy.101), calls=%async_computation.3 | async-start | bytes 4194304 | tf_op jit(solution)/shard_map/all_to_all | solution.py:137
  228.8 1.8 convert_reduce_fusion.1
  230.6 1.2 pad_maximum_fusion
  231.9 95.9 %all-to-all-done.3 = bf16[64,13,1024]{2,1,0:T(8,128)(2,1)} async-done(((bf16[64,13,1024]{2,1,0:T(8,128)(2,1)}), bf16[64,13,1024]{2,1,0:T(8,128)(2,1)}, u32[]{:S(2)}, u32[]{:S(2)}) %all-to-all-start.3) | async-done | bytes 1703968 | tf_op jit(solution)/shard_map/all_to_all | solution.py:137
  327.8 2.6 reshape.131
  330.4 2.9 gather_fusion
  333.3 1.4 gather.7
  334.6 2.1 fusion.1
  (85 shorter events, 11.5 us)
Async XLA Ops:
  7.2 17.1 %copy-start = (bf16[512,2048]{1,0:T(8,128)(2,1)S(1)}, bf16[512,2048]{1,0:T(8,128)(2,1)}, u32[]{:S(2)}) copy-start(bf16[512,2048]{1,0:T(8,128)(2,1)} %param.30) | copy-start | bytes 6291460
  15.7 3.9 %copy-start.17 = (f32[32,64]{1,0:T(8,128)S(1)}, f32[32,64]{1,0:T(8,128)}, u32[]{:S(2)}) copy-start(f32[32,64]{1,0:T(8,128)} %param.25) | copy-start | bytes 24580
  15.7 3.9 %copy-start.18 = (f32[32,64]{1,0:T(8,128)S(1)}, f32[32,64]{1,0:T(8,128)}, u32[]{:S(2)}) copy-start(f32[32,64]{1,0:T(8,128)} %param.24) | copy-start | bytes 24580
  18.2 1.6 copy-start.9
  19.8 3.1 copy-start.14
  22.8 1.0 copy-start.2
  22.9 1.3 copy-start.4
  22.9 1.5 copy-start.20
  24.3 5.3 %copy-start.16 = (s32[96,6]{0,1:T(8,128)S(1)}, s32[96,6]{0,1:T(8,128)}, u32[]{:S(2)}) copy-start(s32[96,6]{0,1:T(8,128)} %param.38) | copy-start | bytes 6916
  25.8 6.8 %copy-start.10 = (bf16[96,2048]{1,0:T(8,128)(2,1)S(1)}, bf16[96,2048]{1,0:T(8,128)(2,1)}, u32[]{:S(2)}) copy-start(bf16[96,2048]{1,0:T(8,128)(2,1)} %param.20) | copy-start | bytes 1179652
  25.8 6.6 %all-to-all-start = ((bf16[2,96,2048]{2,1,0:T(8,128)(2,1)}), bf16[2,96,2048]{2,1,0:T(8,128)(2,1)S(1)}, u32[]{:S(2)}, u32[]{:S(2)}) async-start(bf16[2,96,2048]{2,1,0:T(8,128)(2,1)} %broadcast_in_dim.9), calls=%async_computation | async-start | bytes 1572864 | tf_op jit(solution)/shard_map/all_to_all | solution.py:11
  29.5 152.9 %all-gather.2.cloned.1.call-start = ((), (), s32[]{:S(2)}) async-start(), calls=%async_computation.5 | async-start | bytes 6291456 | tf_op jit(solution)/shard_map/all_gather | solution.py:122
  31.4 2.1 copy-start.15
  32.8 0.7 copy-start.6
  167.5 1.0 copy-start.7
  167.5 2.6 copy-start.12
  167.5 2.6 copy-start.13
  185.9 2.4 copy-start.21
  200.6 10.4 %all-to-all-start.4 = ((bf16[2,96,1024]{2,1,0:T(8,128)(2,1)}), bf16[2,96,1024]{2,1,0:T(8,128)(2,1)}, u32[]{:S(2)}, u32[]{:S(2)}) async-start(bf16[2,96,1024]{2,1,0:T(8,128)(2,1)} %bitcast.89), calls=%async_computation.4 | async-start | bytes 786432 | tf_op jit(solution)/shard_map/all_to_all | solution.py:27
  211.0 16.8 %copy-start.19 = (f32[96,6]{0,1:T(8,128)S(1)}, f32[96,6]{0,1:T(8,128)}, u32[]{:S(2)}) copy-start(f32[96,6]{0,1:T(8,128)} %param.39) | copy-start | bytes 6916
  211.0 17.1 %copy-start.5 = (f32[96,32,64]{0,2,1:T(8,128)S(1)}, f32[96,32,64]{0,2,1:T(8,128)}, u32[]{:S(2)}) copy-start(f32[96,32,64]{0,2,1:T(8,128)} %copy-done.4) | copy-start | bytes 2359300
  211.0 17.4 %copy-start.3 = (f32[96,32,64]{0,2,1:T(8,128)S(1)}, f32[96,32,64]{0,2,1:T(8,128)}, u32[]{:S(2)}) copy-start(f32[96,32,64]{0,2,1:T(8,128)} %copy-done.2) | copy-start | bytes 2359300
  211.0 116.8 %all-to-all-start.3 = ((bf16[64,13,1024]{2,1,0:T(8,128)(2,1)}), bf16[64,13,1024]{2,1,0:T(8,128)(2,1)}, u32[]{:S(2)}, u32[]{:S(2)}) async-start(bf16[64,13,1024]{2,1,0:T(8,128)(2,1)} %copy.101), calls=%async_computation.3 | async-start | bytes 4194304 | tf_op jit(solution)/shard_map/all_to_all | solution.py:137
  333.2 4.3 %copy-start.1 = (bf16[512,2048]{1,0:T(8,128)(2,1)S(1)}, bf16[512,2048]{1,0:T(8,128)(2,1)}, u32[]{:S(2)}) copy-start(bf16[512,2048]{1,0:T(8,128)(2,1)} %param.30) | copy-start | bytes 6291460
  334.6 2.1 copy-start.8
  334.6 2.1 copy-start.11
Sparse Core Ops, SparseCore 0:
  167.7 14.7 all-gather.1
where the time goes:
time: 346 us; the launch traced here: 344 us
  blocking collectives  135 us (39%)
  waiting for transfers between devices  107 us (31%)
  local copies, waits for them, and re-layouts  34.1 us (10%)
  starting transfers between devices  24.5 us (7%)
  matrix products  19.7 us (6%)
  between operations  14.6 us (4%)
  other arithmetic  10.2 us (3%)
    all_to_all x1, blocking collectives, body(): lax.all_to_all(own_cols, 'ep', split_axis=0, concat_axis=0, tiled=True)  128 us
    all_to_all x1, waiting for transfers between devices, body(): lax.all_to_all(summed.astype(jnp.bfloat16), 'ep', split_axis=0, concat_ax...  95.9 us
    all_to_all x1, starting transfers between devices, body(): lax.all_to_all(summed.astype(jnp.bfloat16), 'ep', split_axis=0, concat_ax...  16.5 us
    all_gather x1, waiting for transfers between devices, body(): lax.all_gather(lax.all_to_all(own_cols, 'ep', split_axis=0, concat_axis=0...  10.8 us
  transfers between devices with their start and end apart: 4, of which 2 were waited for; matrix products, arithmetic and copies ran while one was open for 5% of the time, Pallas kernels for 0%

commit v1 on v0

--- a/solution.py
+++ b/solution.py
@@ -119,12 +119,11 @@
     outgoing = outgoing.reshape(experts, slot_cap, -1)
     half_cols = outgoing.shape[2] // lax.axis_size("tp")
     own_cols = lax.dynamic_slice_in_dim(outgoing, lax.axis_index("tp") * half_cols, half_cols, 2)
-    arrived = lax.all_gather(
-        lax.all_to_all(own_cols, "ep", split_axis=0, concat_axis=0, tiled=True),
-        "tp",
-        axis=2,
-        tiled=True,
-    )
+    block = lax.all_to_all(own_cols, "ep", split_axis=0, concat_axis=0, tiled=True)
+    size = lax.axis_size("tp")
+    shards = jnp.stack([block for _ in range(size)])
+    shards = lax.all_to_all(shards, "tp", split_axis=0, concat_axis=0)
+    arrived = jnp.concatenate(shards, axis=2)
     sources, count_items, full_width = arrived.shape
     expert_rows = arrived.reshape(sources * count_items, full_width)
     gate_val = jnp.dot(expert_rows, expert_gate[0], preferred_element_type=jnp.float32)

time: 346 us -> 317 us (0.916)
  blocking collectives: 135 us -> 13 us
  waiting for transfers between devices: 107 us -> 192 us
  starting transfers between devices: 24.5 us -> 42.9 us
  between operations: 14.6 us -> 1.18 us
    all_to_all x1, blocking collectives: 128 us -> 6.49 us  [body(): shards = lax.all_to_all(shards, 'tp', split_axis=0, concat_axis=0)]
    all_to_all x0 -> x1, waiting for transfers between devices: none -> 95.4 us  [body(): lax.all_to_all(own_cols, 'ep', split_axis=0, concat_axis=0, tiled=True)]
    all_to_all x0 -> x1, starting transfers between devices: none -> 28.2 us  [body(): lax.all_to_all(own_cols, 'ep', split_axis=0, concat_axis=0, tiled=True)]
    all_gather x1 -> x0, waiting for transfers between devices: 10.8 us -> none  [body(): lax.all_gather(lax.all_to_all(own_cols, 'ep', split_axis=0, concat_axis=0...]
    all_to_all x1, starting transfers between devices: 16.5 us -> 6.81 us  [body(): lax.all_to_all(summed.astype(jnp.bfloat16), 'ep', split_axis=0, concat_ax...]
  transfers between devices with their start and end apart: 4 -> 4, of which waited for: 2 -> 2; matrix products, arithmetic and copies ran while one was open for 5% -> 6% of each run, Pallas kernels for 0% -> 0%
where the time goes in v1:
time: 317 us; the launch traced here: 315 us
  waiting for transfers between devices  192 us (61%)
  starting transfers between devices  42.9 us (14%)
  local copies, waits for them, and re-layouts  37.1 us (12%)
  matrix products  18.1 us (6%)
  blocking collectives  13 us (4%)
  other arithmetic  11.5 us (4%)
    all_to_all x1, waiting for transfers between devices, body(): lax.all_to_all(summed.astype(jnp.bfloat16), 'ep', split_axis=0, concat_ax...  96.1 us
    all_to_all x1, waiting for transfers between devices, body(): lax.all_to_all(own_cols, 'ep', split_axis=0, concat_axis=0, tiled=True)  95.4 us
    all_to_all x1, starting transfers between devices, body(): lax.all_to_all(own_cols, 'ep', split_axis=0, concat_axis=0, tiled=True)  28.2 us
    all_to_all x1, starting transfers between devices, body(): lax.all_to_all(summed.astype(jnp.bfloat16), 'ep', split_axis=0, concat_ax...  6.81 us
    all_to_all x1, blocking collectives, body(): shards = lax.all_to_all(shards, 'tp', split_axis=0, concat_axis=0)  6.49 us
    all_to_all x1, blocking collectives, summed_on_arrival(): lax.all_to_all(tiles, axis, split_axis=0, concat_axis=0, tiled=True)  6.49 us
  transfers between devices with their start and end apart: 4, of which 2 were waited for; matrix products, arithmetic and copies ran while one was open for 6% of the time, Pallas kernels for 0%

profile of v1, /device:TPU:34, one launch (start us, length us, event | category | flops | bytes accessed | tf_op | source)
XLA Modules:
  0.0 315.3 jit_solution(11936888106509632547)
XLA Ops:
  1.5 1.2 fusion.13
  2.6 2.3 convolution_convert_fusion.4
  5.0 2.7 fusion.72
  7.7 1.5 copy.96
  9.2 2.5 copy.97
  11.7 1.4 fusion.29
  13.3 3.0 bitcast_add_fusion
  19.3 3.7 %all-to-all-start = ((bf16[2,96,2048]{2,1,0:T(8,128)(2,1)}), bf16[2,96,2048]{2,1,0:T(8,128)(2,1)S(1)}, u32[]{:S(2)}, u32[]{:S(2)}) async-start(bf16[2,96,2048]{2,1,0:T(8,128)(2,1)} %broadcast_in_dim.9), calls=%async_computation | async-start | bytes 1572864 | tf_op jit(solution)/shard_map/all_to_all | solution.py:11
  23.3 1.5 reduce-window.6
  27.5 1.1 convolution_convert_fusion.1
  28.6 2.9 reshape.128
  31.5 3.2 %constant_dynamic-slice_fusion = bf16[64,13,1024]{2,1,0:T(8,128)(2,1)} fusion(bf16[64,13,2048]{2,1,0:T(8,128)(2,1)} %reshape.128, s32[]{:T(128)S(6)} %select_n.26), kind=kLoop, calls=%fused_computation.101 | loop fusion | bytes 3407876 | tf_op jit(solution)/shard_map/dynamic_slice | solution.py:121
  34.8 28.2 %all-to-all-start.1 = ((bf16[64,13,1024]{2,1,0:T(8,128)(2,1)}), bf16[64,13,1024]{2,1,0:T(8,128)(2,1)S(1)}, u32[]{:S(2)}, u32[]{:S(2)}) async-start(bf16[64,13,1024]{2,1,0:T(8,128)(2,1)} %constant_dynamic-slice_fusion), calls=%async_computation.1 | async-start | bytes 4194304 | tf_op jit(solution)/shard_map/all_to_all | solution.py:122
  63.0 1.6 fusion.67
  64.7 2.4 convolution_convert_fusion.2
  67.8 95.4 %all-to-all-done.1 = bf16[64,13,1024]{2,1,0:T(8,128)(2,1)S(1)} async-done(((bf16[64,13,1024]{2,1,0:T(8,128)(2,1)}), bf16[64,13,1024]{2,1,0:T(8,128)(2,1)S(1)}, u32[]{:S(2)}, u32[]{:S(2)}) %all-to-all-start.1) | async-done | bytes 1703968 | tf_op jit(solution)/shard_map/all_to_all | solution.py:122
  164.0 2.0 copy.105
  166.0 6.5 %all_to_all.30 = bf16[2,64,13,1024]{3,1,2,0:T(8,128)(2,1)S(1)} all-to-all(bf16[2,64,13,1024]{3,1,2,0:T(8,128)(2,1)S(1)} %copy.105), channel_id=1, replica_groups=mesh['grp'=2,'ep'=64,'tp'=2] {'tp'}, dimensions={0} | all-to-all | bytes 6815744 | tf_op jit(solution)/shard_map/all_to_all | solution.py:125
  172.5 3.5 %copy.106 = bf16[64,13,2,1024]{3,2,1,0:T(2,128)(2,1)S(1)} copy(bf16[64,13,2,1024]{3,0,1,2:T(8,128)(2,1)S(1)} %bitcast.89) | data formatting | bytes 6815744 | tf_op jit(solution)/shard_map/reshape | solution.py:126
  176.0 1.1 copy.122
  181.3 6.5 %all_to_all.31 = bf16[2,64,13,1024]{3,1,2,0:T(8,128)(2,1)S(1)} all-to-all(bf16[2,64,13,1024]{3,1,2,0:T(8,128)(2,1)S(1)} %bitcast.91), channel_id=1, replica_groups=mesh['grp'=2,'ep'=64,'tp'=2] {'tp'}, dimensions={0} | all-to-all | bytes 6815744 | tf_op jit(solution)/shard_map/all_to_all | solution.py:27
  187.8 4.2 %all-to-all-start.5 = ((bf16[2,96,1024]{2,1,0:T(8,128)(2,1)}), bf16[2,96,1024]{2,1,0:T(8,128)(2,1)}, u32[]{:S(2)}, u32[]{:S(2)}) async-start(bf16[2,96,1024]{2,1,0:T(8,128)(2,1)} %bitcast.99), calls=%async_computation.5 | async-start | bytes 786432 | tf_op jit(solution)/shard_map/all_to_all | solution.py:27
  191.9 2.5 reduce_sum.66
  194.4 3.7 %copy.110 = bf16[64,13,1024]{2,1,0:T(8,128)(2,1)} copy(bf16[64,13,1024]{2,0,1:T(8,128)(2,1)} %reduce_sum.66) | data formatting | bytes 3407872 | tf_op jit(solution)/shard_map/reduce_sum | solution.py:28
  198.2 6.8 %all-to-all-start.4 = ((bf16[64,13,1024]{2,1,0:T(8,128)(2,1)}), bf16[64,13,1024]{2,1,0:T(8,128)(2,1)}, u32[]{:S(2)}, u32[]{:S(2)}) async-start(bf16[64,13,1024]{2,1,0:T(8,128)(2,1)} %copy.110), calls=%async_computation.4 | async-start | bytes 4194304 | tf_op jit(solution)/shard_map/all_to_all | solution.py:136
  206.3 1.8 convert_reduce_fusion.1
  208.1 1.2 pad_maximum_fusion.1
  209.4 96.1 %all-to-all-done.4 = bf16[64,13,1024]{2,1,0:T(8,128)(2,1)} async-done(((bf16[64,13,1024]{2,1,0:T(8,128)(2,1)}), bf16[64,13,1024]{2,1,0:T(8,128)(2,1)}, u32[]{:S(2)}, u32[]{:S(2)}) %all-to-all-start.4) | async-done | bytes 1703968 | tf_op jit(solution)/shard_map/all_to_all | solution.py:136
  305.5 2.6 reshape.131
  308.1 2.9 gather_fusion
  311.0 1.4 gather.7
  312.4 2.1 fusion.1
  (93 shorter events, 14.5 us)
Async XLA Ops:
  0.6 17.2 %copy-start = (bf16[512,2048]{1,0:T(8,128)(2,1)S(1)}, bf16[512,2048]{1,0:T(8,128)(2,1)}, u32[]{:S(2)}) copy-start(bf16[512,2048]{1,0:T(8,128)(2,1)} %param.30) | copy-start | bytes 6291460
  9.2 3.9 %copy-start.17 = (f32[32,64]{1,0:T(8,128)S(1)}, f32[32,64]{1,0:T(8,128)}, u32[]{:S(2)}) copy-start(f32[32,64]{1,0:T(8,128)} %param.25) | copy-start | bytes 24580
  9.2 3.9 %copy-start.18 = (f32[32,64]{1,0:T(8,128)S(1)}, f32[32,64]{1,0:T(8,128)}, u32[]{:S(2)}) copy-start(f32[32,64]{1,0:T(8,128)} %param.24) | copy-start | bytes 24580
  11.7 1.6 copy-start.9
  13.3 3.1 copy-start.14
  16.3 1.0 copy-start.2
  16.3 1.3 copy-start.4
  16.3 1.5 copy-start.22
  17.8 5.2 %copy-start.16 = (s32[96,6]{0,1:T(8,128)S(1)}, s32[96,6]{0,1:T(8,128)}, u32[]{:S(2)}) copy-start(s32[96,6]{0,1:T(8,128)} %param.38) | copy-start | bytes 6916
  19.3 7.2 %copy-start.10 = (bf16[96,2048]{1,0:T(8,128)(2,1)S(1)}, bf16[96,2048]{1,0:T(8,128)(2,1)}, u32[]{:S(2)}) copy-start(bf16[96,2048]{1,0:T(8,128)(2,1)} %param.20) | copy-start | bytes 1179652
  19.3 7.1 %all-to-all-start = ((bf16[2,96,2048]{2,1,0:T(8,128)(2,1)}), bf16[2,96,2048]{2,1,0:T(8,128)(2,1)S(1)}, u32[]{:S(2)}, u32[]{:S(2)}) async-start(bf16[2,96,2048]{2,1,0:T(8,128)(2,1)} %broadcast_in_dim.9), calls=%async_computation | async-start | bytes 1572864 | tf_op jit(solution)/shard_map/all_to_all | solution.py:11
  24.8 2.7 copy-start.15
  26.8 0.7 copy-start.6
  26.8 4.8 %copy-start.19 = (f32[96]{0:T(128)}, f32[96]{0:T(128)S(1)}, u32[]{:S(2)}) copy-start(f32[96]{0:T(128)S(1)} %add_rsqrt_fusion) | copy-start | bytes 1156
  34.8 28.3 %copy-start.7 = (bf16[96,2048]{1,0:T(8,128)(2,1)S(1)}, bf16[96,2048]{1,0:T(8,128)(2,1)}, u32[]{:S(2)}) copy-start(bf16[96,2048]{1,0:T(8,128)(2,1)} %copy-done.6) | copy-start | bytes 1179652
  34.8 28.3 %copy-start.13 = (bf16[2048,256]{1,0:T(8,128)(2,1)S(1)}, bf16[2048,256]{1,0:T(8,128)(2,1)}, u32[]{:S(2)}) copy-start(bf16[2048,256]{1,0:T(8,128)(2,1)} %param.35) | copy-start | bytes 3145732
  34.8 128.4 %all-to-all-start.1 = ((bf16[64,13,1024]{2,1,0:T(8,128)(2,1)}), bf16[64,13,1024]{2,1,0:T(8,128)(2,1)S(1)}, u32[]{:S(2)}, u32[]{:S(2)}) async-start(bf16[64,13,1024]{2,1,0:T(8,128)(2,1)} %constant_dynamic-slice_fusion), calls=%async_computation.1 | async-start | bytes 4194304 | tf_op jit(solution)/shard_map/all_to_all | solution.py:122
  176.0 1.2 copy-start.23
  177.2 1.2 copy-start.24
  178.5 1.2 copy-start.12
  187.8 10.4 %all-to-all-start.5 = ((bf16[2,96,1024]{2,1,0:T(8,128)(2,1)}), bf16[2,96,1024]{2,1,0:T(8,128)(2,1)}, u32[]{:S(2)}, u32[]{:S(2)}) async-start(bf16[2,96,1024]{2,1,0:T(8,128)(2,1)} %bitcast.99), calls=%async_computation.5 | async-start | bytes 786432 | tf_op jit(solution)/shard_map/all_to_all | solution.py:27
  198.2 7.1 %copy-start.20 = (f32[96,6]{0,1:T(8,128)S(1)}, f32[96,6]{0,1:T(8,128)}, u32[]{:S(2)}) copy-start(f32[96,6]{0,1:T(8,128)} %param.39) | copy-start | bytes 6916
  198.2 7.3 %copy-start.21 = (pred[96,6]{0,1:T(8,128)(4,1)S(1)}, pred[96,6]{0,1:T(8,128)(4,1)}, u32[]{:S(2)}) copy-start(pred[96,6]{0,1:T(8,128)(4,1)} %get-tuple-element.2) | copy-start | bytes 1732
  198.2 7.4 %copy-start.5 = (f32[96,32,64]{0,2,1:T(8,128)S(1)}, f32[96,32,64]{0,2,1:T(8,128)}, u32[]{:S(2)}) copy-start(f32[96,32,64]{0,2,1:T(8,128)} %copy-done.4) | copy-start | bytes 2359300
  198.2 7.7 %copy-start.3 = (f32[96,32,64]{0,2,1:T(8,128)S(1)}, f32[96,32,64]{0,2,1:T(8,128)}, u32[]{:S(2)}) copy-start(f32[96,32,64]{0,2,1:T(8,128)} %copy-done.2) | copy-start | bytes 2359300
  198.2 107.3 %all-to-all-start.4 = ((bf16[64,13,1024]{2,1,0:T(8,128)(2,1)}), bf16[64,13,1024]{2,1,0:T(8,128)(2,1)}, u32[]{:S(2)}, u32[]{:S(2)}) async-start(bf16[64,13,1024]{2,1,0:T(8,128)(2,1)} %copy.110), calls=%async_computation.4 | async-start | bytes 4194304 | tf_op jit(solution)/shard_map/all_to_all | solution.py:136
  311.0 4.3 %copy-start.1 = (bf16[512,2048]{1,0:T(8,128)(2,1)S(1)}, bf16[512,2048]{1,0:T(8,128)(2,1)}, u32[]{:S(2)}) copy-start(bf16[512,2048]{1,0:T(8,128)(2,1)} %param.30) | copy-start | bytes 6291460
  312.4 2.1 copy-start.8
  312.4 2.1 copy-start.11
